TPU v7x, 32 devices: a whole 2x2x4 slice. The times are simulated.
32 devices in a mesh: fs: 8 (over z, y), tp: 4 (over x, core).
Axes of the slice: x: 2, y: 2, z: 4, core: 2. Of those that a mesh axis runs over, the one named last changes fastest.
Arguments:
- tokens: bfloat16 [4096, 2048], P('fs', 'tp'), may hold values from -6 to 6
- mixer_gain: float32 [2048], replicated, may hold values from 0.1 to 1.9
- recur_in: bfloat16 [2048, 1024], P('fs', 'tp'), may hold values from -0.125 to 0.125
- branch_in: bfloat16 [2048, 1024], P('fs', 'tp'), may hold values from -0.125 to 0.125
- conv_taps: bfloat16 [4, 1024], replicated, may hold values from -3 to 3
- recur_gate: bfloat16 [2, 16, 64, 64], replicated, may hold values from -0.75 to 0.75
- input_gate: bfloat16 [2, 16, 64, 64], replicated, may hold values from -0.75 to 0.75
- decay_param: float32 [2, 1024], replicated, may hold values from 3.5 to 11
- recur_gain: float32 [1024], replicated, may hold values from 0.1 to 1.9
- recur_out: bfloat16 [1024, 2048], P('tp', 'fs'), may hold values from -0.1875 to 0.1875
- mixer_post: float32 [2048], replicated, may hold values from 0.1 to 1.9
- channel_gain: float32 [2048], replicated, may hold values from 0.1 to 1.9
- hidden_gate: bfloat16 [2048, 5632], P('fs', 'tp'), may hold values from -0.125 to 0.125
- hidden_up: bfloat16 [2048, 5632], P('fs', 'tp'), may hold values from -0.125 to 0.125
- hidden_down: bfloat16 [5632, 2048], P('tp', 'fs'), may hold values from -0.078125 to 0.078125
- channel_post: float32 [2048], replicated, may hold values from 0.1 to 1.9
Outputs:
- layer_out: bfloat16 [4096, 2048], P('fs', 'tp')
All inputs are finite; a program needn't handle non-finite values.
Results may differ from a plain program's by a relative error of at most 0.018.
Values may be sent and summed in bfloat16 or wider, within the bound.
A program may use at most 64 MiB of HBM per device.

v0:
```python
import jax
import jax.numpy as jnp
from jax import lax
from jax.sharding import PartitionSpec as P

D = 2048
BLOCK = 64
EPS = 1e-06
SHRINK = 8.0


def rms_scale(values, gain):
    return values * lax.rsqrt(jnp.mean(values * values, axis=-1, keepdims=True) + EPS) * gain


def linear_scan(decay, inflow, reverse):

    def combine(former, latter):
        return (former[0] * latter[0], latter[0] * former[1] + latter[1])

    return lax.associative_scan(combine, (decay, inflow), axis=0, reverse=reverse)[1]


def short_conv(recur_x, taps):
    length = recur_x.shape[0]
    padded = jnp.pad(recur_x.astype(jnp.float32), ((2, 1), (0, 0)))
    total = taps[0] * padded[0:length]
    for position in range(1, taps.shape[0]):
        total = total + taps[position] * padded[position : position + length]
    return total


def recurrence(conv_out, rate_weight, inlet_weight, decay_row, reverse):
    length, width = conv_out.shape
    grouped = conv_out.reshape(length, rate_weight.shape[0], rate_weight.shape[1])
    rate = jax.nn.sigmoid(
        jnp.einsum(
            "lhi,hij->lhj",
            grouped,
            rate_weight.astype(jnp.float32),
            precision=lax.Precision.HIGHEST,
        ).reshape(length, width)
    )
    inlet = jax.nn.sigmoid(
        jnp.einsum(
            "lhi,hij->lhj",
            grouped,
            inlet_weight.astype(jnp.float32),
            precision=lax.Precision.HIGHEST,
        ).reshape(length, width)
    )
    log_decay = -SHRINK * rate * jax.nn.softplus(-decay_row)
    inflow = conv_out * inlet * jnp.sqrt(-jnp.expm1(2.0 * log_decay))
    return linear_scan(jnp.exp(log_decay), inflow, reverse)


def add_slab(source, piece):
    return jnp.dot(source, piece, preferred_element_type=jnp.float32)


def on_device(
    tokens,
    mixer_gain,
    recur_in,
    branch_in,
    conv_taps,
    recur_gate,
    input_gate,
    decay_param,
    recur_gain,
    recur_out,
    mixer_post,
    channel_gain,
    hidden_gate,
    hidden_up,
    hidden_down,
    channel_post,
):
    rank_tp = lax.axis_index("tp")
    feature_width = tokens.shape[1]
    channel_width = recur_in.shape[1]
    group_count = channel_width // BLOCK
    feature_start = rank_tp * feature_width
    channel_start = rank_tp * channel_width
    gathered_in = lax.all_gather(tokens, "tp", axis=1, tiled=True)
    gathered_float = gathered_in.astype(jnp.float32)
    normed_in = rms_scale(gathered_float, mixer_gain).astype(jnp.bfloat16)

    def add_mixer(piece):
        return add_slab(normed_in, piece)

    recur_total = add_mixer(lax.all_gather(recur_in, "fs", axis=0, tiled=True))
    branch_total = add_mixer(lax.all_gather(branch_in, "fs", axis=0, tiled=True))
    recur_x = recur_total.astype(jnp.bfloat16)
    branch_x = branch_total.astype(jnp.bfloat16)
    taps = lax.dynamic_slice_in_dim(conv_taps, channel_start, channel_width, 1).astype(jnp.float32)
    conv_out = short_conv(recur_x, taps)
    group_start = rank_tp * group_count
    rate_own = lax.dynamic_slice_in_dim(recur_gate, group_start, group_count, 1)
    inlet_own = lax.dynamic_slice_in_dim(input_gate, group_start, group_count, 1)
    decay_own = lax.dynamic_slice_in_dim(decay_param, channel_start, channel_width, 1)
    forward = recurrence(conv_out, rate_own[0], inlet_own[0], decay_own[0], False)
    backward = recurrence(conv_out, rate_own[1], inlet_own[1], decay_own[1], True)
    mixed = (forward + backward) * jax.nn.gelu(branch_x.astype(jnp.float32))
    gain_own = lax.dynamic_slice_in_dim(recur_gain, channel_start, channel_width, 0)
    recur_y = (mixed * gain_own).astype(jnp.bfloat16)
    branch_part = jnp.dot(
        recur_y,
        lax.all_gather(recur_out, "fs", axis=1, tiled=True),
        preferred_element_type=jnp.float32,
    )
    branch_sum = lax.psum(branch_part.astype(jnp.bfloat16), "tp").astype(jnp.float32)
    mid_full = (gathered_float + rms_scale(branch_sum, mixer_post)).astype(jnp.bfloat16)
    mid_own = lax.dynamic_slice_in_dim(mid_full, feature_start, feature_width, 1)
    channel_in = rms_scale(mid_full.astype(jnp.float32), channel_gain).astype(jnp.bfloat16)

    def add_channel(piece):
        return add_slab(channel_in, piece)

    gate_total = add_channel(lax.all_gather(hidden_gate, "fs", axis=0, tiled=True))
    up_total = add_channel(lax.all_gather(hidden_up, "fs", axis=0, tiled=True))
    hidden = (jax.nn.silu(gate_total) * up_total).astype(jnp.bfloat16)
    hidden_part = jnp.dot(
        hidden,
        lax.all_gather(hidden_down, "fs", axis=1, tiled=True),
        preferred_element_type=jnp.float32,
    )
    hidden_own = lax.psum_scatter(
        hidden_part.astype(jnp.bfloat16), "tp", scatter_dimension=1, tiled=True
    ).astype(jnp.float32)
    hidden_energy = lax.psum(jnp.sum(hidden_own * hidden_own, axis=1), "tp")
    close_own = lax.dynamic_slice_in_dim(channel_post, feature_start, feature_width, 0)
    return (
        mid_own.astype(jnp.float32)
        + hidden_own * lax.rsqrt(hidden_energy / D + EPS)[:, None] * close_own
    ).astype(jnp.bfloat16)


def solution(mesh):
    in_specs = (
        P("fs", "tp"),
        P(),
        P("fs", "tp"),
        P("fs", "tp"),
        P(),
        P(),
        P(),
        P(),
        P(),
        P("tp", "fs"),
        P(),
        P(),
        P("fs", "tp"),
        P("fs", "tp"),
        P("tp", "fs"),
        P(),
    )
    out_specs = P("fs", "tp")
    return jax.shard_map(
        on_device, mesh=mesh, in_specs=in_specs, out_specs=out_specs, check_vma=False
    )
```

profile of v0, /device:TPU:0, one launch (start us, length us, event | category | flops | bytes accessed | tf_op | source)
XLA Modules:
  0.0 592.1 jit_solution(11456441102849634958)
XLA Ops:
  10.1 1.3 dynamic_slice.25
  12.3 21.9 %all-gather.8.cloned.1.call-done = bf16[512,2048]{1,0:T(8,128)(2,1)} async-done(((bf16[512,512]{1,0:T(8,128)(2,1)}), bf16[512,2048]{1,0:T(8,128)(2,1)}) %all-gather.8.cloned.1.call-update) | async-done | bytes 2097168 | tf_op jit(solution)/shard_map/all_gather | solution.py:85
  34.2 2.1 fusion.5
  36.3 40.3 %all-gather.10.cloned.1.call-done = bf16[2048,256]{1,0:T(8,128)(2,1)} async-done(((bf16[256,256]{1,0:T(8,128)(2,1)}), bf16[2048,256]{1,0:T(8,128)(2,1)}) %all-gather.10.cloned.1.call-update) | async-done | bytes 1048592 | tf_op jit(solution)/shard_map/all_gather | solution.py:92
  76.6 2.6 fusion.22
  80.7 2.1 fusion.21
  82.9 1.3 fusion.17
  85.2 2.0 copy.33
  89.2 2.5 multiply_exponential_fusion
  92.3 1.4 slice.487
  93.7 1.4 slice.485
  95.0 1.4 slice.489
  106.9 1.4 fusion.101
  108.4 1.4 slice.510
  109.7 1.4 slice.511
  111.1 1.4 slice.509
  112.4 1.4 slice.513
  113.8 1.4 fusion.103
  116.4 1.3 slice.515
  117.7 1.3 slice.519
  119.0 1.3 fusion.105
  124.2 1.3 slice.525
  133.3 1.3 fusion.107
  136.5 1.3 slice.537
  139.0 1.3 slice.514
  142.3 1.4 slice.541
  153.2 1.3 slice.561
  165.9 1.4 slice.554
  167.3 1.4 slice.624
  179.0 1.7 pad.132
  181.4 1.7 pad.131
  183.9 1.7 pad.150
  185.6 1.8 slice.555
  187.4 3.0 slice.625
  191.6 1.9 add.409
  193.5 3.4 rev.2
  197.0 5.7 convolution_convert_fusion
  205.1 47.9 %all-reduce.39.cloned.1.call-done = bf16[512,2048]{1,0:T(8,128)(2,1)} async-done(((bf16[512,2048]{1,0:T(8,128)(2,1)}), bf16[512,2048]{1,0:T(8,128)(2,1)}) %all-reduce.39.cloned.1.call-update) | async-done | bytes 2097168 | tf_op jit(solution)/shard_map/psum | solution.py:112
  253.0 2.1 fusion
  255.1 4.0 fusion.2
  259.2 88.3 %all-gather.16.cloned.1.call-done = bf16[2048,1408]{1,0:T(8,128)(2,1)} async-done(((bf16[256,1408]{1,0:T(8,128)(2,1)}), bf16[2048,1408]{1,0:T(8,128)(2,1)}) %all-gather.16.cloned.1.call-update) | async-done | bytes 5767184 | tf_op jit(solution)/shard_map/all_gather | solution.py:120
  347.5 8.5 %fusion.30 = f32[512,1408]{1,0:T(8,128)} fusion(bf16[2048,1408]{1,0:T(8,128)(2,1)} %all-gather.16.cloned.1.call-done, bf16[512,2048]{1,0:T(8,128)(2,1)} %get-tuple-element.6, f32[2048]{0:T(1024)S(1)} %copy-done.23, f32[512]{0:T(512)S(1)} %add_rsqrt_fusion.1), kind=kOutput, calls=%fused_computation.47 | convolution fusion | flops 2956984320 | bytes 10758144 | tf_op jit(solution)/shard_map/dot_general | solution.py:58
  356.0 84.2 %all-gather.18.cloned.1.call-done = bf16[2048,1408]{1,0:T(8,128)(2,1)} async-done(((bf16[256,1408]{1,0:T(8,128)(2,1)}), bf16[2048,1408]{1,0:T(8,128)(2,1)}) %all-gather.18.cloned.1.call-update) | async-done | bytes 5767184 | tf_op jit(solution)/shard_map/all_gather | solution.py:121
  440.2 93.4 %all-gather.20.cloned.1.call-done = bf16[1408,2048]{1,0:T(8,128)(2,1)} async-done(((bf16[1408,256]{1,0:T(8,128)(2,1)}), bf16[1408,2048]{1,0:T(8,128)(2,1)}) %all-gather.20.cloned.1.call-update) | async-done | bytes 5767184 | tf_op jit(solution)/shard_map/all_gather | solution.py:125
  533.6 13.4 %convolution_convert_fusion.1 = bf16[512,2048]{1,0:T(8,128)(2,1)} fusion(bf16[1408,2048]{1,0:T(8,128)(2,1)} %all-gather.20.cloned.1.call-done, bf16[2048,1408]{1,0:T(8,128)(2,1)} %all-gather.18.cloned.1.call-done, f32[512,1408]{1,0:T(8,128)} %fusion.30, bf16[512,2048]{1,0:T(8,128)(2,1)S(1)} %copy-done.2, f32[2048]{0:T(1024)S(1)} %copy-done.23, ...), kind=kOutput, calls=%fused_computation.19 | convolution fusion | flops 5915148288 | bytes 18622464 | tf_op jit(solution)/shard_map/dot_general | solution.py:123
  547.7 28.7 %reduce-scatter.2.cloned.1.call-done = bf16[512,512]{1,0:T(8,128)(2,1)} async-done(((bf16[512,2048]{1,0:T(8,128)(2,1)}), bf16[512,512]{1,0:T(8,128)(2,1)}) %reduce-scatter.2.cloned.1.call-update) | async-done | bytes 524304 | tf_op jit(solution)/shard_map/reduce_scatter | solution.py:128
  577.7 5.8 psum.15
  583.5 2.1 fusion.27
  (269 shorter events, 75.2 us)
Async XLA Ops:
  6.5 73.2 %copy-start = (bf16[2,16,64,64]{3,2,1,0:T(8,128)(2,1)S(1)}, bf16[2,16,64,64]{3,2,1,0:T(8,128)(2,1)}, u32[]{:S(2)}) copy-start(bf16[2,16,64,64]{3,2,1,0:T(8,128)(2,1)} %param.22) | copy-start | bytes 786436
  6.5 27.7 %all-gather.8.cloned.1.call-start = ((), (), s32[]{:S(2)}) async-start(), calls=%async_computation.1 | async-start | bytes 2621440 | tf_op jit(solution)/shard_map/all_gather | solution.py:85
  7.3 69.4 %all-gather.10.cloned.1.call-start = ((), (), s32[]{:S(2)}) async-start(), calls=%async_computation.2 | async-start | bytes 1179648 | tf_op jit(solution)/shard_map/all_gather | solution.py:92
  8.0 189.0 %all-gather.12.cloned.1.call-start = ((), (), s32[]{:S(2)}) async-start(), calls=%async_computation.3 | async-start | bytes 1179648 | tf_op jit(solution)/shard_map/all_gather | solution.py:93
  8.7 188.2 %all-gather.14.cloned.1.call-start = ((), (), s32[]{:S(2)}) async-start(), calls=%async_computation.4 | async-start | bytes 1179648 | tf_op jit(solution)/shard_map/all_gather | solution.py:109
  9.3 243.7 %all-reduce.39.cloned.1.call-start = ((), (), s32[]{:S(2)}) async-start(), calls=%async_computation.5 | async-start | bytes 4194304 | tf_op jit(solution)/shard_map/psum | solution.py:112
  36.3 43.0 %copy-start.19 = (f32[512]{0:T(512)}, f32[512]{0:T(512)S(1)}, u32[]{:S(2)}) copy-start(f32[512]{0:T(512)S(1)} %add_rsqrt_fusion.3) | copy-start | bytes 6148
  155.7 22.4 %copy-start.3 = (f32[127,256]{1,0:T(8,128)S(1)}, f32[127,256]{1,0:T(8,128)}, u32[]{:S(2)}) copy-start(f32[127,256]{1,0:T(8,128)} %slice.547) | copy-start | bytes 390148
  168.7 14.4 %copy-start.17 = (f32[1,256]{1,0:T(1,128)S(1)}, f32[1,256]{1,0:T(1,128)}, u32[]{:S(2)}) copy-start(f32[1,256]{1,0:T(1,128)} %get-tuple-element.41) | copy-start | bytes 3076
  168.7 14.4 %copy-start.18 = (f32[1,256]{1,0:T(1,128)S(1)}, f32[1,256]{1,0:T(1,128)}, u32[]{:S(2)}) copy-start(f32[1,256]{1,0:T(1,128)} %get-tuple-element.42) | copy-start | bytes 3076
  168.7 14.4 %copy-start.9 = (f32[2,256]{1,0:T(2,128)S(1)}, f32[2,256]{1,0:T(2,128)}, u32[]{:S(2)}) copy-start(f32[2,256]{1,0:T(2,128)} %pad_add_fusion) | copy-start | bytes 6148
  170.0 13.2 %copy-start.6 = (f32[3,256]{1,0:T(4,128)S(1)}, f32[3,256]{1,0:T(4,128)}, u32[]{:S(2)}) copy-start(f32[3,256]{1,0:T(4,128)} %slice.595) | copy-start | bytes 9220
  170.0 13.2 %copy-start.7 = (f32[3,256]{1,0:T(4,128)S(1)}, f32[3,256]{1,0:T(4,128)}, u32[]{:S(2)}) copy-start(f32[3,256]{1,0:T(4,128)} %slice.612) | copy-start | bytes 9220
  170.7 12.6 %copy-start.16 = (f32[1,256]{1,0:T(1,128)S(1)}, f32[1,256]{1,0:T(1,128)}, u32[]{:S(2)}) copy-start(f32[1,256]{1,0:T(1,128)} %slice.666) | copy-start | bytes 3076
  172.0 11.2 %copy-start.4 = (f32[7,256]{1,0:T(8,128)S(1)}, f32[7,256]{1,0:T(8,128)}, u32[]{:S(2)}) copy-start(f32[7,256]{1,0:T(8,128)} %slice.589) | copy-start | bytes 21508
  172.0 11.2 %copy-start.5 = (f32[7,256]{1,0:T(8,128)S(1)}, f32[7,256]{1,0:T(8,128)}, u32[]{:S(2)}) copy-start(f32[7,256]{1,0:T(8,128)} %slice.614) | copy-start | bytes 21508
  172.1 11.2 %copy-start.15 = (f32[1,256]{1,0:T(1,128)S(1)}, f32[1,256]{1,0:T(1,128)}, u32[]{:S(2)}) copy-start(f32[1,256]{1,0:T(1,128)} %slice.665) | copy-start | bytes 3076
  174.2 9.2 %copy-start.14 = (f32[1,256]{1,0:T(1,128)S(1)}, f32[1,256]{1,0:T(1,128)}, u32[]{:S(2)}) copy-start(f32[1,256]{1,0:T(1,128)} %slice.664) | copy-start | bytes 3076
  175.7 7.8 %copy-start.13 = (f32[1,256]{1,0:T(1,128)S(1)}, f32[1,256]{1,0:T(1,128)}, u32[]{:S(2)}) copy-start(f32[1,256]{1,0:T(1,128)} %slice.663) | copy-start | bytes 3076
  177.4 6.2 %copy-start.12 = (f32[1,256]{1,0:T(1,128)S(1)}, f32[1,256]{1,0:T(1,128)}, u32[]{:S(2)}) copy-start(f32[1,256]{1,0:T(1,128)} %slice.662) | copy-start | bytes 3076
  178.2 5.6 copy-start.11
  183.1 8.4 %copy-start.10 = (f32[1,256]{1,0:T(1,128)S(1)}, f32[1,256]{1,0:T(1,128)}, u32[]{:S(2)}) copy-start(f32[1,256]{1,0:T(1,128)} %slice.660) | copy-start | bytes 3076
  183.8 13.2 %copy-start.1 = (bf16[512,2048]{1,0:T(8,128)(2,1)S(1)}, bf16[512,2048]{1,0:T(8,128)(2,1)}, u32[]{:S(2)}) copy-start(bf16[512,2048]{1,0:T(8,128)(2,1)} %all-gather.8.cloned.1.call-done) | copy-start | bytes 6291460
  183.8 13.2 %copy-start.20 = (f32[512]{0:T(512)S(1)}, f32[512]{0:T(512)}, u32[]{:S(2)}) copy-start(f32[512]{0:T(512)} %copy-done.19) | copy-start | bytes 6148
  183.8 13.2 %copy-start.21 = (f32[256]{0:T(256)S(1)}, f32[256]{0:T(256)}, u32[]{:S(2)}) copy-start(f32[256]{0:T(256)} %dynamic_slice.25) | copy-start | bytes 3076
  183.8 13.2 %copy-start.22 = (f32[2048]{0:T(1024)S(1)}, f32[2048]{0:T(1024)}, u32[]{:S(2)}) copy-start(f32[2048]{0:T(1024)} %param.17) | copy-start | bytes 24580
  202.7 52.4 %copy-start.8 = (f32[2048]{0:T(1024)S(1)}, f32[2048]{0:T(1024)}, u32[]{:S(2)}) copy-start(f32[2048]{0:T(1024)} %param.26) | copy-start | bytes 24580
  202.8 144.7 %all-gather.16.cloned.1.call-start = ((), (), s32[]{:S(2)}) async-start(), calls=%async_computation.6 | async-start | bytes 6488064 | tf_op jit(solution)/shard_map/all_gather | solution.py:120
  203.3 236.9 %all-gather.18.cloned.1.call-start = ((), (), s32[]{:S(2)}) async-start(), calls=%async_computation.7 | async-start | bytes 6488064 | tf_op jit(solution)/shard_map/all_gather | solution.py:121
  204.1 329.5 %all-gather.20.cloned.1.call-start = ((), (), s32[]{:S(2)}) async-start(), calls=%async_computation.8 | async-start | bytes 6488064 | tf_op jit(solution)/shard_map/all_gather | solution.py:125
  204.8 142.7 %copy-start.23 = (f32[2048]{0:T(1024)S(1)}, f32[2048]{0:T(1024)}, u32[]{:S(2)}) copy-start(f32[2048]{0:T(1024)} %param.27) | copy-start | bytes 24580
  204.8 371.6 %reduce-scatter.2.cloned.1.call-start = ((), (), s32[]{:S(2)}) async-start(), calls=%async_computation.9 | async-start | bytes 2621440 | tf_op jit(solution)/shard_map/reduce_scatter | solution.py:128
  347.5 186.1 %copy-start.2 = (bf16[512,2048]{1,0:T(8,128)(2,1)S(1)}, bf16[512,2048]{1,0:T(8,128)(2,1)}, u32[]{:S(2)}) copy-start(bf16[512,2048]{1,0:T(8,128)(2,1)} %get-tuple-element.6) | copy-start | bytes 6291460
Sparse Core Ops, SparseCore 0:
  8.9 25.2 all-gather.7
  36.3 40.2 all-gather.9
  78.8 38.9 all-gather.11
  119.7 38.0 all-gather.13
  202.9 50.1 all-reduce.38
  255.1 92.3 all-gather.15
  349.7 90.4 all-gather.17
  442.2 91.2 all-gather.19
  547.1 29.3 reduce-scatter.1
where the time goes:
time: 595 us; the launch traced here: 592 us
  waiting for transfers between devices  409 us (69%)
  local copies, waits for them, and re-layouts  84 us (14%)
  other arithmetic  43.5 us (7%)
  matrix products  34.6 us (6%)
  between operations  14.2 us (2%)
    all_gather x1, waiting for transfers between devices, on_device(): lax.all_gather(hidden_down, 'fs', axis=1, tiled=True)  93.4 us
    all_gather x1, waiting for transfers between devices, on_device(): lax.all_gather(hidden_gate, 'fs', axis=0, tiled=True)  88.3 us
    all_gather x1, waiting for transfers between devices, on_device(): up_total = add_channel(lax.all_gather(hidden_up, 'fs', axis=0, tiled=True))  84.2 us
    slice x112, local copies, waits for them, and re-layouts, linear_scan(): lax.associative_scan(combine, (decay, inflow), axis=0, reverse=reverse)[1]  66.9 us
    psum x1, waiting for transfers between devices, on_device(): lax.psum(branch_part.astype(jnp.bfloat16), 'tp').astype(jnp.float32)  47.9 us
    all_gather x1, waiting for transfers between devices, on_device(): recur_total = add_mixer(lax.all_gather(recur_in, 'fs', axis=0, tiled=True))  40.3 us
    reduce_scatter x1, waiting for transfers between devices, on_device(): lax.psum_scatter(hidden_part.astype(jnp.bfloat16), 'tp', scatter_dimensio...  28.7 us
    all_gather x1, waiting for transfers between devices, on_device(): gathered_in = lax.all_gather(tokens, 'tp', axis=1, tiled=True)  21.9 us
  transfers between devices with their start and end apart: 9, of which 7 were waited for; matrix products, arithmetic and copies ran while one was open for 24% of the time, Pallas kernels for 0%

commit v1 on v0

--- a/solution.py
+++ b/solution.py
@@ -7,6 +7,11 @@
 BLOCK = 64
 EPS = 1e-06
 SHRINK = 8.0
+
+
+def all_parts(block, name, along):
+    blocks = lax.all_gather(block, name)
+    return jnp.concatenate(blocks, axis=along)
 
 
 def rms_scale(values, gain):
@@ -121,9 +126,7 @@
     up_total = add_channel(lax.all_gather(hidden_up, "fs", axis=0, tiled=True))
     hidden = (jax.nn.silu(gate_total) * up_total).astype(jnp.bfloat16)
     hidden_part = jnp.dot(
-        hidden,
-        lax.all_gather(hidden_down, "fs", axis=1, tiled=True),
-        preferred_element_type=jnp.float32,
+        hidden, all_parts(hidden_down, "fs", 1), preferred_element_type=jnp.float32
     )
     hidden_own = lax.psum_scatter(
         hidden_part.astype(jnp.bfloat16), "tp", scatter_dimension=1, tiled=True

time: 595 us -> 554 us (0.931)
  local copies, waits for them, and re-layouts: 84 us -> 47.9 us
  other arithmetic: 43.5 us -> 26.8 us
  waiting for transfers between devices: 409 us -> 424 us
    slice x112, local copies, waits for them, and re-layouts: 66.9 us -> 24.9 us  [linear_scan(): lax.associative_scan(combine, (decay, inflow), axis=0, reverse=reverse)[1]]
    all_gather x1, waiting for transfers between devices: 0.02 us -> 21.9 us  [on_device(): lax.all_gather(recur_out, 'fs', axis=1, tiled=True)]
    mul x14, other arithmetic: 10.6 us -> 1.28 us  [combine(): return (former[0] * latter[0], latter[0] * former[1] + latter[1])]
    reshape x0 -> x1, local copies, waits for them, and re-layouts: none -> 8.33 us  [all_parts(): return jnp.concatenate(blocks, axis=along)]
  transfers between devices with their start and end apart: 9 -> 9, of which waited for: 7 -> 8; matrix products, arithmetic and copies ran while one was open for 24% -> 16% of each run, Pallas kernels for 0% -> 0%
where the time goes in v1:
time: 554 us; the launch traced here: 552 us
  waiting for transfers between devices  424 us (77%)
  local copies, waits for them, and re-layouts  47.9 us (9%)
  matrix products  33.7 us (6%)
  other arithmetic  26.8 us (5%)
  between operations  14.3 us (3%)
  blocking collectives  5.76 us (1%)
    all_gather x1, waiting for transfers between devices, all_parts(): blocks = lax.all_gather(block, name)  88.3 us
    all_gather x1, waiting for transfers between devices, on_device(): up_total = add_channel(lax.all_gather(hidden_up, 'fs', axis=0, tiled=True))  85 us
    all_gather x1, waiting for transfers between devices, on_device(): lax.all_gather(hidden_gate, 'fs', axis=0, tiled=True)  84.4 us
    psum x1, waiting for transfers between devices, on_device(): lax.psum(branch_part.astype(jnp.bfloat16), 'tp').astype(jnp.float32)  48.4 us
    all_gather x1, waiting for transfers between devices, on_device(): recur_total = add_mixer(lax.all_gather(recur_in, 'fs', axis=0, tiled=True))  40.3 us
    reduce_scatter x1, waiting for transfers between devices, on_device(): lax.psum_scatter(hidden_part.astype(jnp.bfloat16), 'tp', scatter_dimensio...  28.7 us
    slice x112, local copies, waits for them, and re-layouts, linear_scan(): lax.associative_scan(combine, (decay, inflow), axis=0, reverse=reverse)[1]  24.9 us
    all_gather x1, waiting for transfers between devices, on_device(): gathered_in = lax.all_gather(tokens, 'tp', axis=1, tiled=True)  22 us
  transfers between devices with their start and end apart: 9, of which 8 were waited for; matrix products, arithmetic and copies ran while one was open for 16% of the time, Pallas kernels for 0%

profile of v1, /device:TPU:0, one launch (start us, length us, event | category | flops | bytes accessed | tf_op | source)
XLA Modules:
  0.0 552.4 jit_solution(5989394387770745416)
XLA Ops:
  6.5 0.7 all-gather.9.cloned.1.call-update
  7.3 0.7 all-gather.11.cloned.1.call-update
  10.1 1.3 dynamic_slice.25
  11.4 0.8 fusion.85
  12.2 22.0 %all-gather.9.cloned.1.call-done = bf16[512,2048]{1,0:T(8,128)(2,1)} async-done(((bf16[512,512]{1,0:T(8,128)(2,1)}), bf16[512,2048]{1,0:T(8,128)(2,1)}) %all-gather.9.cloned.1.call-update) | async-done | bytes 2097168 | tf_op jit(solution)/shard_map/all_gather | solution.py:90
  34.2 2.1 fusion.5
  36.3 40.3 %all-gather.11.cloned.1.call-done = bf16[2048,256]{1,0:T(8,128)(2,1)} async-done(((bf16[256,256]{1,0:T(8,128)(2,1)}), bf16[2048,256]{1,0:T(8,128)(2,1)}) %all-gather.11.cloned.1.call-update) | async-done | bytes 1048592 | tf_op jit(solution)/shard_map/all_gather | solution.py:97
  76.6 2.6 fusion.22
  80.8 2.1 fusion.21
  82.9 1.3 fusion.17
  84.4 2.1 copy.40
  86.5 1.0 copy.36
  87.5 1.0 copy.38
  88.5 2.3 multiply_exponential_fusion
  92.1 1.4 slice.489
  93.5 1.0 fusion.95
  110.3 1.4 slice.554
  111.7 1.4 slice.624
  114.4 0.7 pad.118
  115.1 0.7 fusion.75
  116.5 0.7 fusion.73
  117.9 0.7 fusion.71
  119.3 0.8 fusion.69
  121.2 1.7 pad.132
  122.9 1.7 pad.131
  125.5 2.0 slice.555
  127.5 3.0 slice.625
  130.5 1.0 fusion.57
  131.7 0.9 add.409
  132.5 3.4 rev.2
  136.0 21.9 %all-gather.15.cloned.1.call-done = bf16[256,2048]{1,0:T(8,128)(2,1)} async-done(((bf16[256,256]{1,0:T(8,128)(2,1)}), bf16[256,2048]{1,0:T(8,128)(2,1)}) %all-gather.15.cloned.1.call-update) | async-done | bytes 1048592 | tf_op jit(solution)/shard_map/all_gather | solution.py:114
  157.9 5.6 %convolution_convert_fusion = bf16[512,2048]{1,0:T(8,128)(2,1)} fusion(bf16[256,2048]{1,0:T(8,128)(2,1)} %all-gather.15.cloned.1.call-done, bf16[2048,256]{1,0:T(8,128)(2,1)} %all-gather.13.cloned.1.call-done, bf16[512,2048]{1,0:T(8,128)(2,1)S(1)} %copy-done.2, f32[2048]{0:T(1024)S(1)} %copy-done.12, f32[512]{0:T(512)S(1)} %copy-done.10, ...), kind=kOutput, calls=%fused_computation.17 | convolution fusion | flops 1080950784 | bytes 7875584 | tf_op jit(solution)/shard_map/dot_general | solution.py:112
  164.1 0.7 all-gather.17.cloned.1.call-update
  164.9 0.7 all-gather.19.cloned.1.call-update
  165.6 48.4 %all-reduce.39.cloned.1.call-done = bf16[512,2048]{1,0:T(8,128)(2,1)} async-done(((bf16[512,2048]{1,0:T(8,128)(2,1)}), bf16[512,2048]{1,0:T(8,128)(2,1)}) %all-reduce.39.cloned.1.call-update) | async-done | bytes 2097168 | tf_op jit(solution)/shard_map/psum | solution.py:117
  214.1 2.1 fusion
  216.2 4.1 fusion.2
  220.3 88.3 %all-gather.21.cloned.1.call-done = bf16[11264,256]{1,0:T(8,128)(2,1)} async-done(((bf16[1408,256]{1,0:T(8,128)(2,1)}), bf16[11264,256]{1,0:T(8,128)(2,1)}) %all-gather.21.cloned.1.call-update) | async-done | bytes 5767184 | tf_op jit(solution)/shard_map/all_gather | solution.py:13
  308.5 8.3 %copy.41 = bf16[1408,8,256]{0,2,1:T(8,128)(2,1)} copy(bf16[1408,8,256]{2,0,1:T(8,128)(2,1)} %bitcast.49) | data formatting | bytes 11534336 | tf_op jit(solution)/shard_map/reshape | solution.py:14
  316.9 84.4 %all-gather.17.cloned.1.call-done = bf16[2048,1408]{1,0:T(8,128)(2,1)} async-done(((bf16[256,1408]{1,0:T(8,128)(2,1)}), bf16[2048,1408]{1,0:T(8,128)(2,1)}) %all-gather.17.cloned.1.call-update) | async-done | bytes 5767184 | tf_op jit(solution)/shard_map/all_gather | solution.py:125
  401.2 7.7 %fusion.30 = f32[512,1408]{1,0:T(8,128)} fusion(bf16[2048,1408]{1,0:T(8,128)(2,1)} %all-gather.17.cloned.1.call-done, bf16[512,2048]{1,0:T(8,128)(2,1)S(1)} %copy-done.3, f32[2048]{0:T(1024)S(1)} %copy-done.13, f32[512]{0:T(512)S(1)} %add_rsqrt_fusion.1), kind=kOutput, calls=%fused_computation.47 | convolution fusion | flops 2956984320 | bytes 10758144 | tf_op jit(solution)/shard_map/dot_general | solution.py:63
  408.9 85.0 %all-gather.19.cloned.1.call-done = bf16[2048,1408]{1,0:T(8,128)(2,1)} async-done(((bf16[256,1408]{1,0:T(8,128)(2,1)}), bf16[2048,1408]{1,0:T(8,128)(2,1)}) %all-gather.19.cloned.1.call-update) | async-done | bytes 5767184 | tf_op jit(solution)/shard_map/all_gather | solution.py:126
  493.9 13.3 %convolution_convert_fusion.1 = bf16[512,2048]{1,0:T(8,128)(2,1)} fusion(bf16[1408,2048]{0,1:T(8,128)(2,1)} %bitcast.50, bf16[2048,1408]{1,0:T(8,128)(2,1)} %all-gather.19.cloned.1.call-done, f32[512,1408]{1,0:T(8,128)} %fusion.30, bf16[512,2048]{1,0:T(8,128)(2,1)S(1)} %copy-done.3, f32[2048]{0:T(1024)S(1)} %copy-done.13, f32[512]{0:T(512)S(1)} %add_rsqrt_fusion.1), kind=kOutput, calls=%fused_computation.19 | convolution fusion | flops 5915148288 | bytes 18622464 | tf_op jit(solution)/shard_map/dot_general | solution.py:128
  507.3 0.8 dynamic_slice.27
  508.0 28.7 %reduce-scatter.2.cloned.1.call-done = bf16[512,512]{1,0:T(8,128)(2,1)} async-done(((bf16[512,2048]{1,0:T(8,128)(2,1)}), bf16[512,512]{1,0:T(8,128)(2,1)}) %reduce-scatter.2.cloned.1.call-update) | async-done | bytes 524304 | tf_op jit(solution)/shard_map/reduce_scatter | solution.py:131
  536.8 1.2 fusion.24
  538.0 5.8 %psum.15 = f32[512]{0:T(512)S(1)} all-reduce(f32[512]{0:T(512)S(1)} %fusion.24), channel_id=1, replica_groups=mesh['fs'=8,'tp'=4] {'tp'}, use_global_device_ids=true, to_apply=%region_6.7 | all-reduce | flops 512 | bytes 4096 | tf_op jit(solution)/shard_map/psum | solution.py:134
  543.7 2.1 fusion.27
  (250 shorter events, 26.1 us)
Async XLA Ops:
  6.5 73.2 %copy-start = (bf16[2,16,64,64]{3,2,1,0:T(8,128)(2,1)S(1)}, bf16[2,16,64,64]{3,2,1,0:T(8,128)(2,1)}, u32[]{:S(2)}) copy-start(bf16[2,16,64,64]{3,2,1,0:T(8,128)(2,1)} %param.22) | copy-start | bytes 786436
  6.5 27.7 %all-gather.9.cloned.1.call-start = ((), (), s32[]{:S(2)}) async-start(), calls=%async_computation.1 | async-start | bytes 2621440 | tf_op jit(solution)/shard_map/all_gather | solution.py:90
  7.3 69.4 %all-gather.11.cloned.1.call-start = ((), (), s32[]{:S(2)}) async-start(), calls=%async_computation.2 | async-start | bytes 1179648 | tf_op jit(solution)/shard_map/all_gather | solution.py:97
  8.0 128.0 %all-gather.13.cloned.1.call-start = ((), (), s32[]{:S(2)}) async-start(), calls=%async_computation.3 | async-start | bytes 1179648 | tf_op jit(solution)/shard_map/all_gather | solution.py:98
  8.7 149.1 %all-gather.15.cloned.1.call-start = ((), (), s32[]{:S(2)}) async-start(), calls=%async_computation.4 | async-start | bytes 1179648 | tf_op jit(solution)/shard_map/all_gather | solution.py:114
  9.3 204.7 %all-reduce.39.cloned.1.call-start = ((), (), s32[]{:S(2)}) async-start(), calls=%async_computation.5 | async-start | bytes 4194304 | tf_op jit(solution)/shard_map/psum | solution.py:117
  36.3 43.9 %copy-start.9 = (f32[512]{0:T(512)}, f32[512]{0:T(512)S(1)}, u32[]{:S(2)}) copy-start(f32[512]{0:T(512)S(1)} %add_rsqrt_fusion.3) | copy-start | bytes 6148
  108.4 12.5 %copy-start.7 = (f32[1,256]{1,0:T(1,128)S(1)}, f32[1,256]{1,0:T(1,128)}, u32[]{:S(2)}) copy-start(f32[1,256]{1,0:T(1,128)} %slice.632) | copy-start | bytes 3076
  108.6 12.4 %copy-start.6 = (f32[1,256]{1,0:T(1,128)S(1)}, f32[1,256]{1,0:T(1,128)}, u32[]{:S(2)}) copy-start(f32[1,256]{1,0:T(1,128)} %slice.631) | copy-start | bytes 3076
  110.1 12.8 %copy-start.5 = (f32[1,256]{1,0:T(1,128)S(1)}, f32[1,256]{1,0:T(1,128)}, u32[]{:S(2)}) copy-start(f32[1,256]{1,0:T(1,128)} %slice.630) | copy-start | bytes 3076
  124.7 6.9 %copy-start.8 = (f32[1,256]{1,0:T(1,128)S(1)}, f32[1,256]{1,0:T(1,128)}, u32[]{:S(2)}) copy-start(f32[1,256]{1,0:T(1,128)} %slice.660) | copy-start | bytes 3076
  125.3 32.6 %copy-start.2 = (bf16[512,2048]{1,0:T(8,128)(2,1)S(1)}, bf16[512,2048]{1,0:T(8,128)(2,1)}, u32[]{:S(2)}) copy-start(bf16[512,2048]{1,0:T(8,128)(2,1)} %all-gather.9.cloned.1.call-done) | copy-start | bytes 6291460
  125.3 32.6 %copy-start.10 = (f32[512]{0:T(512)S(1)}, f32[512]{0:T(512)}, u32[]{:S(2)}) copy-start(f32[512]{0:T(512)} %copy-done.9) | copy-start | bytes 6148
  125.3 32.6 %copy-start.11 = (f32[256]{0:T(256)S(1)}, f32[256]{0:T(256)}, u32[]{:S(2)}) copy-start(f32[256]{0:T(256)} %dynamic_slice.25) | copy-start | bytes 3076
  125.3 32.5 %copy-start.12 = (f32[2048]{0:T(1024)S(1)}, f32[2048]{0:T(1024)}, u32[]{:S(2)}) copy-start(f32[2048]{0:T(1024)} %param.17) | copy-start | bytes 24580
  163.5 52.7 %copy-start.4 = (f32[2048]{0:T(1024)S(1)}, f32[2048]{0:T(1024)}, u32[]{:S(2)}) copy-start(f32[2048]{0:T(1024)} %param.26) | copy-start | bytes 24580
  163.5 145.0 %all-gather.21.cloned.1.call-start = ((), (), s32[]{:S(2)}) async-start(), calls=%async_computation.9 | async-start | bytes 6488064 | tf_op jit(solution)/shard_map/all_gather | solution.py:13
  164.1 237.1 %all-gather.17.cloned.1.call-start = ((), (), s32[]{:S(2)}) async-start(), calls=%async_computation.6 | async-start | bytes 6488064 | tf_op jit(solution)/shard_map/all_gather | solution.py:125
  164.8 329.1 %all-gather.19.cloned.1.call-start = ((), (), s32[]{:S(2)}) async-start(), calls=%async_computation.7 | async-start | bytes 6488064 | tf_op jit(solution)/shard_map/all_gather | solution.py:126
  165.6 371.2 %reduce-scatter.2.cloned.1.call-start = ((), (), s32[]{:S(2)}) async-start(), calls=%async_computation.8 | async-start | bytes 2621440 | tf_op jit(solution)/shard_map/reduce_scatter | solution.py:131
  308.5 92.7 %copy-start.3 = (bf16[512,2048]{1,0:T(8,128)(2,1)S(1)}, bf16[512,2048]{1,0:T(8,128)(2,1)}, u32[]{:S(2)}) copy-start(bf16[512,2048]{1,0:T(8,128)(2,1)} %get-tuple-element.6) | copy-start | bytes 6291460
  308.5 92.7 %copy-start.13 = (f32[2048]{0:T(1024)S(1)}, f32[2048]{0:T(1024)}, u32[]{:S(2)}) copy-start(f32[2048]{0:T(1024)} %param.27) | copy-start | bytes 24580
  493.9 51.9 %copy-start.1 = (bf16[2,16,64,64]{3,2,1,0:T(8,128)(2,1)S(1)}, bf16[2,16,64,64]{3,2,1,0:T(8,128)(2,1)}, u32[]{:S(2)}) copy-start(bf16[2,16,64,64]{3,2,1,0:T(8,128)(2,1)} %param.22) | copy-start | bytes 786436
Sparse Core Ops, SparseCore 0:
  8.9 25.2 all-gather.8
  36.3 40.2 all-gather.10
  78.8 38.9 all-gather.12
  119.7 38.0 all-gather.14
  163.6 50.3 all-reduce.38
  216.1 92.3 all-gather.20
  310.7 90.4 all-gather.16
  403.4 90.4 all-gather.18
  507.4 29.3 reduce-scatter.1
